TPU v7x, 32 devices: a whole 2x2x4 slice. The times are simulated.
32 devices in a mesh: sp: 8 (over z, x), tp: 4 (over y, core).
Axes of the slice: x: 2, y: 2, z: 4, core: 2. Of those that a mesh axis runs over, the one named last changes fastest.
Arguments:
- features: bfloat16 [3072, 2048], P('sp', 'tp'), may hold values from -6 to 6
- norm_gain: float32 [2048], replicated, may hold values from 0.28 to 10
- w_query: bfloat16 [2048, 1024], P(None, 'tp'), may hold values from -0.125 to 0.125
- w_key: bfloat16 [2048, 512], P(None, 'tp'), may hold values from -0.125 to 0.125
- w_value: bfloat16 [2048, 512], P(None, 'tp'), may hold values from -0.125 to 0.125
- head_sinks: float32 [16], P('tp'), may hold values from 1 to 5
- w_query_latent: bfloat16 [2048, 512], replicated, may hold values from -0.125 to 0.125
- w_kv_latent: bfloat16 [2048, 512], replicated, may hold values from -0.125 to 0.125
- w_rope_key: bfloat16 [2048, 64], replicated, may hold values from -0.125 to 0.125
- query_latent_gain: float32 [512], replicated, may hold values from 0.28 to 10
- kv_latent_gain: float32 [512], replicated, may hold values from 0.28 to 10
- w_query_content: bfloat16 [512, 1024], P(None, 'tp'), may hold values from -0.25 to 0.25
- w_query_rotary: bfloat16 [512, 512], P(None, 'tp'), may hold values from -0.25 to 0.25
- w_key_up: bfloat16 [512, 1024], P(None, 'tp'), may hold values from -0.25 to 0.25
- w_value_up: bfloat16 [512, 1024], P(None, 'tp'), may hold values from -0.25 to 0.25
- w_branch_window: bfloat16 [1024, 2048], P('tp'), may hold values from -0.1875 to 0.1875
- w_branch_latent: bfloat16 [1024, 2048], P('tp'), may hold values from -0.1875 to 0.1875
- w_gate_window: bfloat16 [2048, 2048], P(None, 'tp'), may hold values from -0.125 to 0.125
- w_gate_latent: bfloat16 [2048, 2048], P(None, 'tp'), may hold values from -0.125 to 0.125
Outputs:
- mixed: bfloat16 [3072, 2048], P('sp', 'tp')
All inputs are finite; a program needn't handle non-finite values.
Results may differ from a plain program's by a relative error of at most 0.018.
The roundings to bfloat16 on the way count: a program that leaves them out, or rounds other values in their place, can miss the bound.
Values may be sent and summed in bfloat16 or wider, within the bound.
A program may use at most 128 MiB of HBM per device.

v0:
```python
import jax
import jax.numpy as jnp
from jax import lax
from jax.sharding import PartitionSpec as P

HEAD = 64
WINDOW = 128
NOPE = 128
ROPE = 64
VDIM = 128
EPS = 1e-06
THETA = 10000.0
NEGATIVE = -1e30


def from_behind(shard, axis, by):
    count = lax.axis_size(axis)
    pairs = [(i, i + by) for i in range(count) if 0 <= i + by < count]
    return lax.ppermute(shard, axis, pairs)


def rms_rows(float_rows, gain_vec):
    return (
        float_rows
        * lax.rsqrt(jnp.mean(float_rows * float_rows, axis=-1, keepdims=True) + EPS)
        * gain_vec
    )


def rotate(float_rows, positions):
    half_width = float_rows.shape[-1] // 2
    frequencies = THETA ** (-jnp.arange(half_width, dtype=jnp.float32) / half_width)
    angles = positions.astype(jnp.float32)[:, None] * frequencies
    target = (float_rows.shape[0],) + (1,) * (float_rows.ndim - 2) + (half_width,)
    cosine = jnp.cos(angles).reshape(target)
    sine_part = jnp.sin(angles).reshape(target)
    first_half = float_rows[..., :half_width]
    second_half = float_rows[..., half_width:]
    return jnp.concatenate(
        [
            first_half * cosine - second_half * sine_part,
            second_half * cosine + first_half * sine_part,
        ],
        axis=-1,
    )


def project(left, right):
    return jnp.dot(left, right, preferred_element_type=jnp.float32)


def window_attention(queries, key_ext, value_ext, sink_table, row_start):
    row_count = queries.shape[0]
    kv_heads = key_ext.shape[1] // HEAD
    group_size = queries.shape[1] // HEAD // kv_heads
    blocks = row_count // WINDOW
    query_blocks = queries.reshape(blocks, WINDOW, kv_heads, group_size, HEAD)

    def banded(table):
        table = table.reshape(blocks + 1, WINDOW, kv_heads, HEAD)
        return jnp.concatenate([table[:-1], table[1:]], axis=1)

    key_band = banded(key_ext)
    value_band = banded(value_ext)
    scores = jnp.einsum(
        "nqhgd,nkhd->nhgqk", query_blocks, key_band, preferred_element_type=jnp.float32
    ) * HEAD ** (-0.5)
    query_index = jnp.arange(WINDOW, dtype=jnp.int32)[:, None]
    key_index = jnp.arange(2 * WINDOW, dtype=jnp.int32)[None, :]
    offset = query_index + WINDOW - key_index
    key_position = (
        row_start + jnp.arange(blocks, dtype=jnp.int32)[:, None, None] * WINDOW + key_index - WINDOW
    )
    valid_mask = ((offset >= 0) & (offset < WINDOW) & (key_position >= 0))[:, None, None]
    scores = jnp.where(valid_mask, scores, NEGATIVE)
    sink_logit = sink_table.reshape(1, kv_heads, group_size, 1, 1)
    row_top = jnp.maximum(jnp.max(scores, axis=-1, keepdims=True), sink_logit)
    weights = jnp.where(valid_mask, jnp.exp(scores - row_top), 0.0)
    denominator = jnp.sum(weights, axis=-1, keepdims=True) + jnp.exp(sink_logit - row_top)
    probabilities = (weights / denominator).astype(jnp.bfloat16)
    attended = jnp.einsum(
        "nhgqk,nkhd->nqhgd", probabilities, value_band, preferred_element_type=jnp.float32
    )
    return attended.astype(jnp.bfloat16).reshape(row_count, kv_heads * group_size * HEAD)


def on_device(
    features,
    norm_gain,
    w_query,
    w_key,
    w_value,
    head_sinks,
    w_query_latent,
    w_kv_latent,
    w_rope_key,
    query_latent_gain,
    kv_latent_gain,
    w_query_content,
    w_query_rotary,
    w_key_up,
    w_value_up,
    w_branch_window,
    w_branch_latent,
    w_gate_window,
    w_gate_latent,
):
    tok_rows = features.shape[0]
    row_start = lax.axis_index("sp") * tok_rows
    row_end = row_start + tok_rows
    positions = row_start + jnp.arange(tok_rows, dtype=jnp.int32)
    gathered = lax.all_gather(features, "tp", axis=1, tiled=True)
    normed = rms_rows(gathered.astype(jnp.float32), norm_gain).astype(jnp.bfloat16)
    query_rows = project(normed, w_query).astype(jnp.bfloat16)
    key_rows = project(normed, w_key).astype(jnp.bfloat16)
    value_rows = project(normed, w_value).astype(jnp.bfloat16)
    key_width = key_rows.shape[1]
    packed = jnp.concatenate([key_rows, value_rows], axis=1)
    tail_rows = from_behind(packed[tok_rows - WINDOW :], "sp", 1)
    extended = jnp.concatenate([tail_rows, packed], axis=0)
    window_out = window_attention(
        query_rows, extended[:, :key_width], extended[:, key_width:], head_sinks, row_start
    )
    latent_query = rms_rows(project(normed, w_query_latent), query_latent_gain).astype(jnp.bfloat16)
    latent_kv = rms_rows(project(normed, w_kv_latent), kv_latent_gain).astype(jnp.bfloat16)
    rope_rows = rotate(project(normed, w_rope_key), positions).astype(jnp.bfloat16)
    lat_heads = w_key_up.shape[1] // NOPE
    query_content = (
        project(latent_query, w_query_content)
        .astype(jnp.bfloat16)
        .reshape(tok_rows, lat_heads, NOPE)
    )
    query_rotary = rotate(
        project(latent_query, w_query_rotary).reshape(tok_rows, lat_heads, ROPE), positions
    ).astype(jnp.bfloat16)
    scale_factor = (NOPE + ROPE) ** (-0.5)

    def attend(running, piece_keys, piece_values, rope_piece):
        running_max, denominator, accumulated = running
        piece_rows = piece_keys.shape[0]
        scores = (
            jnp.einsum(
                "qhd,khd->hqk",
                query_content,
                piece_keys.reshape(piece_rows, lat_heads, NOPE),
                preferred_element_type=jnp.float32,
            )
            + jnp.einsum(
                "qhr,kr->hqk", query_rotary, rope_piece, preferred_element_type=jnp.float32
            )
        ) * scale_factor
        key_position = jnp.arange(piece_rows, dtype=jnp.int32)
        live_mask = key_position[None, :] <= positions[:, None]
        scores = jnp.where(live_mask, scores, NEGATIVE)
        new_max = jnp.maximum(running_max, jnp.max(scores, axis=-1))
        weights = jnp.where(live_mask, jnp.exp(scores - new_max[..., None]), 0.0)
        denominator = jnp.sum(weights, axis=-1)
        accumulated = jnp.einsum(
            "hqk,khd->hqd",
            weights.astype(jnp.bfloat16),
            piece_values.reshape(piece_rows, lat_heads, VDIM),
            preferred_element_type=jnp.float32,
        )
        return (new_max, denominator, accumulated)

    initial = (
        jnp.full((lat_heads, tok_rows), NEGATIVE, jnp.float32),
        jnp.zeros((lat_heads, tok_rows), jnp.float32),
        jnp.zeros((lat_heads, tok_rows, VDIM), jnp.float32),
    )
    pieces = (
        lax.all_gather(latent_kv, "sp", axis=0, tiled=True),
        lax.all_gather(rope_rows, "sp", axis=0, tiled=True),
    )

    def compute(current):
        piece_keys = project(pieces[0], w_key_up).astype(jnp.bfloat16)
        piece_values = project(pieces[0], w_value_up).astype(jnp.bfloat16)
        return attend(current, piece_keys, piece_values, pieces[1])

    running = lax.cond(jnp.int32(0) < row_end, compute, lambda current: current, initial)
    latent_out = jnp.transpose(running[2] / running[1][..., None], (1, 0, 2))
    latent_out = latent_out.reshape(tok_rows, lat_heads * VDIM).astype(jnp.bfloat16)
    all_window, all_latent = (
        lax.all_gather(window_out, "tp", axis=1, tiled=True),
        lax.all_gather(latent_out, "tp", axis=1, tiled=True),
    )
    column_window, column_latent = (
        lax.all_to_all(w_branch_window, "tp", split_axis=1, concat_axis=0, tiled=True),
        lax.all_to_all(w_branch_latent, "tp", split_axis=1, concat_axis=0, tiled=True),
    )
    window_branch = project(all_window, column_window)
    latent_branch = project(all_latent, column_latent)
    window_gate = jax.nn.sigmoid(project(normed, w_gate_window))
    latent_gate = jax.nn.sigmoid(project(normed, w_gate_latent))
    return (window_gate * window_branch + latent_gate * latent_branch).astype(jnp.bfloat16)


def solution(mesh):
    return jax.shard_map(
        on_device,
        mesh=mesh,
        in_specs=(
            P("sp", "tp"),
            P(),
            P(None, "tp"),
            P(None, "tp"),
            P(None, "tp"),
            P("tp"),
            P(),
            P(),
            P(),
            P(),
            P(),
            P(None, "tp"),
            P(None, "tp"),
            P(None, "tp"),
            P(None, "tp"),
            P("tp", None),
            P("tp", None),
            P(None, "tp"),
            P(None, "tp"),
        ),
        out_specs=P("sp", "tp"),
        check_vma=False,
    )
```

profile of v0, /device:TPU:0, one launch (start us, length us, event | category | flops | bytes accessed | tf_op | source)
XLA Modules:
  0.0 168.1 jit_solution(3678124389484324087)
XLA Ops:
  7.3 2.3 %copy.60 = bf16[256,2048]{0,1:T(8,128)(2,1)} copy(bf16[256,2048]{1,0:T(8,128)(2,1)} %param.37) | data formatting | bytes 2097152 | tf_op args[16]
  9.5 4.4 %all-to-all-start.1 = ((bf16[256,4,512]{0,2,1:T(8,128)(2,1)}), bf16[256,4,512]{0,2,1:T(8,128)(2,1)S(1)}, u32[]{:S(2)}, u32[]{:S(2)}) async-start(bf16[256,4,512]{0,2,1:T(8,128)(2,1)} %bitcast.96), calls=%async_computation.1 | async-start | bytes 2097152 | tf_op jit(solution)/shard_map/all_to_all | solution.py:190
  14.0 2.3 %copy.57 = bf16[256,2048]{0,1:T(8,128)(2,1)} copy(bf16[256,2048]{1,0:T(8,128)(2,1)} %param.36) | data formatting | bytes 2097152 | tf_op args[15]
  16.3 19.8 %all-to-all-done.1 = bf16[256,4,512]{0,2,1:T(8,128)(2,1)S(1)} async-done(((bf16[256,4,512]{0,2,1:T(8,128)(2,1)}), bf16[256,4,512]{0,2,1:T(8,128)(2,1)S(1)}, u32[]{:S(2)}, u32[]{:S(2)}) %all-to-all-start.1) | async-done | bytes 1048608 | tf_op jit(solution)/shard_map/all_to_all | solution.py:190
  36.1 4.2 %all-to-all-start = ((bf16[256,4,512]{0,2,1:T(8,128)(2,1)}), bf16[256,4,512]{0,2,1:T(8,128)(2,1)}, u32[]{:S(2)}, u32[]{:S(2)}) async-start(bf16[256,4,512]{0,2,1:T(8,128)(2,1)} %bitcast.97), calls=%async_computation | async-start | bytes 2097152 | tf_op jit(solution)/shard_map/all_to_all | solution.py:189
  40.7 1.3 copy.61
  42.0 12.8 %all-to-all-done = bf16[256,4,512]{0,2,1:T(8,128)(2,1)} async-done(((bf16[256,4,512]{0,2,1:T(8,128)(2,1)}), bf16[256,4,512]{0,2,1:T(8,128)(2,1)}, u32[]{:S(2)}, u32[]{:S(2)}) %all-to-all-start) | async-done | bytes 1048608 | tf_op jit(solution)/shard_map/all_to_all | solution.py:189
  54.8 2.3 %copy.58 = bf16[4,256,512]{2,1,0:T(8,128)(2,1)} copy(bf16[4,256,512]{1,2,0:T(8,128)(2,1)} %bitcast.12) | data formatting | bytes 2097152 | tf_op jit(solution)/shard_map/all_to_all | solution.py:189
  57.1 1.9 %fusion.14 = f32[384]{0:T(512)S(1)} fusion(bf16[384,2048]{1,0:T(8,128)(2,1)} %all-gather.3.cloned.1.call-done), kind=kLoop, calls=%fused_computation.22 | loop fusion | flops 2358912 | bytes 1574400 | tf_op jit(solution)/shard_map/reduce_sum | solution.py:25
  59.5 1.1 multiply_reduce_fusion.1
  61.7 2.0 %convolution_convert_fusion.6 = bf16[384,128]{0,1:T(8,128)(2,1)S(1)} fusion(bf16[384,2048]{1,0:T(8,128)(2,1)} %copy-done.2, bf16[2048,128]{1,0:T(8,128)(2,1)S(1)} %copy-done.12), kind=kOutput, calls=%fused_computation.46 | convolution fusion | flops 201375744 | bytes 2195456 | tf_op jit(solution)/shard_map/dot_general | solution.py:49
  63.8 2.0 %convolution_convert_fusion.5 = bf16[384,128]{0,1:T(8,128)(2,1)S(1)} fusion(bf16[384,2048]{1,0:T(8,128)(2,1)} %copy-done.2, bf16[2048,128]{1,0:T(8,128)(2,1)S(1)} %copy-done.13), kind=kOutput, calls=%fused_computation.45 | convolution fusion | flops 201375744 | bytes 2195456 | tf_op jit(solution)/shard_map/dot_general | solution.py:49
  66.5 5.2 %collective-permute-start = (bf16[128,256]{0,1:T(8,128)(2,1)}, bf16[128,256]{0,1:T(8,128)(2,1)}, u32[]{:S(2)}, u32[]{:S(2)}) collective-permute-start(bf16[128,256]{0,1:T(8,128)(2,1)} %pad_maximum_fusion.4), channel_id=1, source_target_pairs={{0,4},{4,8},{8,12},{12,16},{16,20},{20,24},{24,28},{1,5},{5,9},{9,... | collective-permute-start | bytes 196616 | tf_op jit(solution)/shard_map/ppermute | solution.py:19
  72.3 2.3 %convolution_convert_fusion.3 = bf16[384,256]{1,0:T(8,128)(2,1)S(1)} fusion(bf16[384,2048]{1,0:T(8,128)(2,1)} %copy-done.2, bf16[2048,256]{1,0:T(8,128)(2,1)} %param.23), kind=kOutput, calls=%fused_computation.42 | convolution fusion | flops 402751488 | bytes 2818048 | tf_op jit(solution)/shard_map/dot_general | solution.py:49
  74.9 2.1 %fusion.41 = f32[384,64]{0,1:T(8,128)S(1)} fusion(bf16[384,2048]{1,0:T(8,128)(2,1)} %copy-done.2, bf16[2048,64]{0,1:T(8,128)(2,1)S(1)} %copy-done.18), kind=kOutput, calls=%fused_computation.93 | convolution fusion | flops 100663296 | bytes 1933312 | tf_op jit(solution)/shard_map/dot_general | solution.py:49
  77.3 35.1 %all_gather.18 = bf16[3072,64]{0,1:T(8,128)(2,1)} all-gather(bf16[384,64]{0,1:T(8,128)(2,1)S(1)} %pad_maximum_fusion.5), channel_id=1, replica_groups=mesh['sp'=8,'tp'=4] {'sp'}, dimensions={0}, use_global_device_ids=true | all-gather | bytes 442368 | tf_op jit(solution)/shard_map/all_gather | solution.py:173
  112.5 2.7 %multiply_reduce_fusion = (f32[384]{0:T(512)S(1)}, f32[384,512]{1,0:T(8,128)S(1)}) fusion(bf16[384,2048]{1,0:T(8,128)(2,1)S(1)} %copy-done.3, bf16[2048,512]{1,0:T(8,128)(2,1)} %param.27), kind=kOutput, calls=%fused_computation.48 | convolution fusion | flops 805699200 | bytes 4457984 | tf_op jit(solution)/shard_map/dot_general | solution.py:49
  116.1 1.0 convolution_convert_fusion.2
  117.1 2.0 %fusion.24 = f32[384,512]{1,0:T(8,128)} fusion(bf16[384,2048]{1,0:T(8,128)(2,1)S(1)} %copy-done.3, bf16[2048,512]{1,0:T(8,128)(2,1)S(1)} %copy-done.24), kind=kOutput, calls=%fused_computation.39 | convolution fusion | flops 805896192 | bytes 4456448 | tf_op jit(solution)/shard_map/dot_general | solution.py:49
  119.1 2.0 %fusion.22 = f32[384,512]{1,0:T(8,128)} fusion(bf16[384,2048]{1,0:T(8,128)(2,1)S(1)} %copy-done.3, bf16[2048,512]{1,0:T(8,128)(2,1)S(1)} %copy-done.25), kind=kOutput, calls=%fused_computation.37 | convolution fusion | flops 805896192 | bytes 4456448 | tf_op jit(solution)/shard_map/dot_general | solution.py:49
  124.3 7.9 %all_gather.16 = bf16[384,1024]{0,1:T(8,128)(2,1)} all-gather(bf16[384,256]{0,1:T(8,128)(2,1)S(1)} %bitcast.100), channel_id=1, replica_groups=mesh['sp'=8,'tp'=4] {'tp'}, dimensions={1}, use_global_device_ids=true | all-gather | bytes 983040 | tf_op jit(solution)/shard_map/all_gather | solution.py:185
  132.2 15.7 %conditional.1 = (f32[2,384]{1,0:T(2,128)S(1)}, f32[2,384,128]{1,2,0:T(8,128)}) conditional(s32[]{:T(128)} %convert_element_type.75, () %tuple.13, (s32[]{:T(128)}, s32[384]{0:T(512)S(1)}, bf16[3072,512]{1,0:T(8,128)(2,1)}, bf16[512,256]{1,0:T(8,128)(2,1)S(1)}, bf16[384,256]{1,0:T(8,128)(2,1)}, /*index=5*/bf16[3072,64]{0,1:T(8,128)(2,1)}, ...), branch_computations={%region_5.6_spmd, %region_6.9_spmd} | conditional | flops 3146907136 | bytes 87218872 | solution.py:181
  133.1 3.4 %convolution_convert_fusion.1 = bf16[3072,256]{0,1:T(8,128)(2,1)S(1)} fusion(bf16[3072,512]{1,0:T(8,128)(2,1)} %get-tuple-element.26, bf16[512,256]{1,0:T(8,128)(2,1)S(1)} %get-tuple-element.38), kind=kOutput, calls=%fused_computation.12 | convolution fusion | flops 806092800 | bytes 4980736 | tf_op jit(solution)/shard_map/cond/branch_1_fun/dot_general | solution.py:49
  136.5 1.6 fusion.10
  138.1 2.4 %fusion.39 = (f32[2,384]{1,0:T(2,128)S(1)}, f32[2,384,3072]{1,2,0:T(8,128)S(1)}) fusion(bf16[384,2,64]{0,2,1:T(8,128)(2,1)S(1)} %copy-done.14, bf16[3072,64]{0,1:T(8,128)(2,1)S(1)} %copy-done.9, f32[2,3072,384]{2,1,0:T(8,128)S(1)} %fusion.10, pred[384,3072]{0,1:T(8,128)(4,1)S(1)} %iota_compare_fusion), kind=kOutput, calls=%fused_computation.91 | convolution fusion | flops 311426304 | bytes 20548608 | tf_op jit(solution)/shard_map/cond/branch_1_fun/qhr,kr->hqk/dot_general | solution.py:148
  140.5 1.0 convolution_convert_fusion
  141.6 3.1 %fusion.4 = f32[2,384,128]{1,2,0:T(8,128)} fusion(bf16[3072,2,128]{0,2,1:T(8,128)(2,1)S(1)} %bitcast.93, f32[2,384,3072]{1,2,0:T(8,128)S(1)} %get-tuple-element.42, f32[2,384]{1,0:T(2,128)S(1)} %broadcast_maximum_fusion, pred[384,3072]{0,1:T(8,128)(4,1)S(1)} %iota_compare_fusion), kind=kOutput, calls=%fused_computation.6 | convolution fusion | flops 611057664 | bytes 12585984 | tf_op jit(solution)/shard_map/cond | solution.py:181
  144.7 3.2 %fusion.3 = f32[2,384]{1,0:T(2,128)S(1)} fusion(f32[2,384,3072]{1,2,0:T(8,128)S(1)} %get-tuple-element.42, f32[2,384]{1,0:T(2,128)S(1)} %broadcast_maximum_fusion, pred[384,3072]{0,1:T(8,128)(4,1)} %copy-done.4), kind=kLoop, calls=%fused_computation.5 | loop fusion | flops 7077120 | bytes 10622976 | tf_op jit(solution)/shard_map/cond/branch_1_fun/reduce_sum | solution.py:157
  147.9 1.1 divide_convert_fusion.2
  149.0 9.0 %all_gather.19 = bf16[384,1024]{0,1:T(8,128)(2,1)S(1)} all-gather(bf16[384,256]{0,1:T(8,128)(2,1)S(1)} %bitcast.102), channel_id=1, replica_groups=mesh['sp'=8,'tp'=4] {'tp'}, dimensions={1}, use_global_device_ids=true | all-gather | bytes 983040 | tf_op jit(solution)/shard_map/all_gather | solution.py:186
  158.0 1.9 %convolution_multiply_fusion = f32[384,512]{1,0:T(8,128)S(1)} fusion(f32[384,512]{1,0:T(8,128)} %fusion.24, bf16[384,1024]{0,1:T(8,128)(2,1)S(1)} %all_gather.19, bf16[1024,512]{1,0:T(8,128)(2,1)S(1)} %bitcast.94), kind=kOutput, calls=%fused_computation.28 | convolution fusion | flops 402849792 | bytes 3407872 | tf_op jit(solution)/shard_map/dot_general | solution.py:49
  159.9 1.4 fusion.25
  (101 shorter events, 9.6 us)
Async XLA Ops:
  6.5 53.0 %copy-start = (bf16[2048,512]{1,0:T(8,128)(2,1)S(1)}, bf16[2048,512]{1,0:T(8,128)(2,1)}, u32[]{:S(2)}) copy-start(bf16[2048,512]{1,0:T(8,128)(2,1)} %param.28) | copy-start | bytes 6291460
  6.5 50.6 %all-gather.3.cloned.1.call-start = ((), (), s32[]{:S(2)}) async-start(), calls=%async_computation.2 | async-start | bytes 1966080 | tf_op jit(solution)/shard_map/all_gather | solution.py:112
  9.5 4.4 %copy-start.26 = (f32[4]{0:T(128)S(1)}, f32[4]{0:T(128)}, u32[]{:S(2)}) copy-start(f32[4]{0:T(128)} %param.26) | copy-start | bytes 52
  9.5 26.6 %all-to-all-start.1 = ((bf16[256,4,512]{0,2,1:T(8,128)(2,1)}), bf16[256,4,512]{0,2,1:T(8,128)(2,1)S(1)}, u32[]{:S(2)}, u32[]{:S(2)}) async-start(bf16[256,4,512]{0,2,1:T(8,128)(2,1)} %bitcast.96), calls=%async_computation.1 | async-start | bytes 2097152 | tf_op jit(solution)/shard_map/all_to_all | solution.py:190
  36.1 18.7 %all-to-all-start = ((bf16[256,4,512]{0,2,1:T(8,128)(2,1)}), bf16[256,4,512]{0,2,1:T(8,128)(2,1)}, u32[]{:S(2)}, u32[]{:S(2)}) async-start(bf16[256,4,512]{0,2,1:T(8,128)(2,1)} %bitcast.97), calls=%async_computation | async-start | bytes 2097152 | tf_op jit(solution)/shard_map/all_to_all | solution.py:189
  40.3 91.8 %all-gather.5.cloned.1.call-start = ((), (), s32[]{:S(2)}) async-start(), calls=%async_computation.3 | async-start | bytes 3538944 | tf_op jit(solution)/shard_map/all_gather | solution.py:172
  54.8 4.2 %copy-start.21 = (f32[2048]{0:T(1024)S(1)}, f32[2048]{0:T(1024)}, u32[]{:S(2)}) copy-start(f32[2048]{0:T(1024)} %param.22) | copy-start | bytes 24580
  57.1 1.9 %copy-start.5 = (bf16[384,2048]{1,0:T(8,128)(2,1)S(1)}, bf16[384,2048]{1,0:T(8,128)(2,1)}, u32[]{:S(2)}) copy-start(bf16[384,2048]{1,0:T(8,128)(2,1)} %all-gather.3.cloned.1.call-done) | copy-start | bytes 4718596
  59.5 1.2 copy-start.2
  59.5 1.2 copy-start.23
  60.7 1.0 copy-start.12
  61.6 2.2 %copy-start.13 = (bf16[2048,128]{1,0:T(8,128)(2,1)S(1)}, bf16[2048,128]{1,0:T(8,128)(2,1)}, u32[]{:S(2)}) copy-start(bf16[2048,128]{1,0:T(8,128)(2,1)} %param.25) | copy-start | bytes 1572868
  66.5 55.2 %collective-permute-start = (bf16[128,256]{0,1:T(8,128)(2,1)}, bf16[128,256]{0,1:T(8,128)(2,1)}, u32[]{:S(2)}, u32[]{:S(2)}) collective-permute-start(bf16[128,256]{0,1:T(8,128)(2,1)} %pad_maximum_fusion.4), channel_id=1, source_target_pairs={{0,4},{4,8},{8,12},{12,16},{16,20},{20,24},{24,28},{1,5},{5,9},{9,... | collective-permute-start | bytes 196616 | tf_op jit(solution)/shard_map/ppermute | solution.py:19
  72.3 2.6 %copy-start.18 = (bf16[2048,64]{0,1:T(8,128)(2,1)S(1)}, bf16[2048,64]{0,1:T(8,128)(2,1)}, u32[]{:S(2)}) copy-start(bf16[2048,64]{0,1:T(8,128)(2,1)} %param.29) | copy-start | bytes 786436
  74.9 37.6 %copy-start.3 = (bf16[384,2048]{1,0:T(8,128)(2,1)S(1)}, bf16[384,2048]{1,0:T(8,128)(2,1)}, u32[]{:S(2)}) copy-start(bf16[384,2048]{1,0:T(8,128)(2,1)} %copy-done.2) | copy-start | bytes 4718596
  112.4 2.7 %copy-start.19 = (bf16[512,128]{1,0:T(8,128)(2,1)S(1)}, bf16[512,128]{1,0:T(8,128)(2,1)}, u32[]{:S(2)}) copy-start(bf16[512,128]{1,0:T(8,128)(2,1)} %param.33) | copy-start | bytes 393220
  112.4 2.7 %copy-start.22 = (f32[512]{0:T(512)S(1)}, f32[512]{0:T(512)}, u32[]{:S(2)}) copy-start(f32[512]{0:T(512)} %param.30) | copy-start | bytes 6148
  115.1 1.0 copy-start.15
  115.1 1.9 %copy-start.24 = (bf16[2048,512]{1,0:T(8,128)(2,1)S(1)}, bf16[2048,512]{1,0:T(8,128)(2,1)}, u32[]{:S(2)}) copy-start(bf16[2048,512]{1,0:T(8,128)(2,1)} %param.39) | copy-start | bytes 6291460
  117.1 2.0 %copy-start.25 = (bf16[2048,512]{1,0:T(8,128)(2,1)S(1)}, bf16[2048,512]{1,0:T(8,128)(2,1)}, u32[]{:S(2)}) copy-start(bf16[2048,512]{1,0:T(8,128)(2,1)} %param.38) | copy-start | bytes 6291460
  121.0 1.6 copy-start.20
  124.0 8.1 %copy-start.16 = (bf16[512,256]{1,0:T(8,128)(2,1)S(1)}, bf16[512,256]{1,0:T(8,128)(2,1)}, u32[]{:S(2)}) copy-start(bf16[512,256]{1,0:T(8,128)(2,1)} %param.34) | copy-start | bytes 786436
  133.1 8.5 %copy-start.4 = (pred[384,3072]{0,1:T(8,128)(4,1)}, pred[384,3072]{0,1:T(8,128)(4,1)S(1)}, u32[]{:S(2)}) copy-start(pred[384,3072]{0,1:T(8,128)(4,1)S(1)} %iota_compare_fusion) | copy-start | bytes 3538948 | tf_op jit(solution)/shard_map/cond
  133.1 3.4 %copy-start.11 = (bf16[384,256]{1,0:T(8,128)(2,1)S(1)}, bf16[384,256]{1,0:T(8,128)(2,1)}, u32[]{:S(2)}) copy-start(bf16[384,256]{1,0:T(8,128)(2,1)} %get-tuple-element.28) | copy-start | bytes 589828 | tf_op jit(solution)/shard_map/cond
  136.5 1.6 copy-start.9
  136.5 1.6 copy-start.14
  138.1 2.5 %copy-start.1 = (bf16[3072,512]{1,0:T(8,128)(2,1)S(1)}, bf16[3072,512]{1,0:T(8,128)(2,1)}, u32[]{:S(2)}) copy-start(bf16[3072,512]{1,0:T(8,128)(2,1)} %get-tuple-element.26) | copy-start | bytes 9437188 | tf_op jit(solution)/shard_map/cond
  138.1 2.5 %copy-start.17 = (bf16[512,256]{1,0:T(8,128)(2,1)S(1)}, bf16[512,256]{1,0:T(8,128)(2,1)}, u32[]{:S(2)}) copy-start(bf16[512,256]{1,0:T(8,128)(2,1)} %get-tuple-element.39) | copy-start | bytes 786436 | tf_op jit(solution)/shard_map/cond
  147.9 10.1 %copy-start.6 = (bf16[4,256,512]{2,1,0:T(8,128)(2,1)S(1)}, bf16[4,256,512]{2,1,0:T(8,128)(2,1)}, u32[]{:S(2)}) copy-start(bf16[4,256,512]{2,1,0:T(8,128)(2,1)} %copy.61) | copy-start | bytes 3145732
  158.0 1.9 %copy-start.7 = (bf16[4,256,512]{2,1,0:T(8,128)(2,1)S(1)}, bf16[4,256,512]{2,1,0:T(8,128)(2,1)}, u32[]{:S(2)}) copy-start(bf16[4,256,512]{2,1,0:T(8,128)(2,1)} %copy.58) | copy-start | bytes 3145732
  158.0 1.9 %copy-start.8 = (bf16[384,1024]{0,1:T(8,128)(2,1)S(1)}, bf16[384,1024]{0,1:T(8,128)(2,1)}, u32[]{:S(2)}) copy-start(bf16[384,1024]{0,1:T(8,128)(2,1)} %all_gather.16) | copy-start | bytes 2359300
  158.0 1.9 %copy-start.10 = (f32[384,512]{1,0:T(8,128)S(1)}, f32[384,512]{1,0:T(8,128)}, u32[]{:S(2)}) copy-start(f32[384,512]{1,0:T(8,128)} %fusion.22) | copy-start | bytes 2359300
Sparse Core Ops, SparseCore 0:
  8.9 29.3 all-gather.2
  61.7 65.5 all-gather.4
where the time goes:
time: 169 us; the launch traced here: 168 us
  blocking collectives  52 us (31%)
  waiting for transfers between devices  33.3 us (20%)
  matrix products  33.2 us (20%)
  starting transfers between devices  13.9 us (8%)
  between operations  13.7 us (8%)
  other arithmetic  11.6 us (7%)
  local copies, waits for them, and re-layouts  10.3 us (6%)
    all_gather x1, blocking collectives, on_device(): lax.all_gather(rope_rows, 'sp', axis=0, tiled=True)  35.1 us
    dot_general x14, matrix products, project(): return jnp.dot(left, right, preferred_element_type=jnp.float32)  25.1 us
    all_to_all x1, waiting for transfers between devices, on_device(): lax.all_to_all(w_branch_latent, 'tp', split_axis=1, concat_axis=0, tiled=...  19.8 us
    all_to_all x1, waiting for transfers between devices, on_device(): lax.all_to_all(w_branch_window, 'tp', split_axis=1, concat_axis=0, tiled=...  12.8 us
    all_gather x1, blocking collectives, on_device(): lax.all_gather(latent_out, 'tp', axis=1, tiled=True)  8.98 us
    all_gather x1, blocking collectives, on_device(): lax.all_gather(window_out, 'tp', axis=1, tiled=True)  7.89 us
    unnamed x45, local copies, waits for them, and re-layouts  5.36 us
    ppermute x1, starting transfers between devices, from_behind(): return lax.ppermute(shard, axis, pairs)  5.23 us
  transfers between devices with their start and end apart: 5, of which 2 were waited for; matrix products, arithmetic and copies ran while one was open for 18% of the time, Pallas kernels for 0%

commit v1 on v0

--- a/solution.py
+++ b/solution.py
@@ -186,7 +186,12 @@
         lax.all_gather(latent_out, "tp", axis=1, tiled=True),
     )
     column_window, column_latent = (
-        lax.all_to_all(w_branch_window, "tp", split_axis=1, concat_axis=0, tiled=True),
+        jnp.concatenate(
+            lax.all_to_all(
+                jnp.stack(jnp.split(w_branch_window, lax.axis_size("tp"), axis=1)), "tp", 0, 0
+            ),
+            axis=0,
+        ),
         lax.all_to_all(w_branch_latent, "tp", split_axis=1, concat_axis=0, tiled=True),
     )
     window_branch = project(all_window, column_window)

time: 169 us -> 157 us (0.929)
  waiting for transfers between devices: 33.3 us -> 20.1 us
  local copies, waits for them, and re-layouts: 10.3 us -> 6.99 us
  matrix products: 33.2 us -> 35.8 us
    all_to_all x1, waiting for transfers between devices: 12.8 us -> 0.01 us  [on_device(): lax.all_to_all(jnp.stack(jnp.split(w_branch_window, lax.axis_size('tp'),...]
    dot_general x14, matrix products: 25.1 us -> 27.7 us  [project(): return jnp.dot(left, right, preferred_element_type=jnp.float32)]
    all_to_all x1 -> x0, local copies, waits for them, and re-layouts: 2.28 us -> none  [on_device(): lax.all_to_all(w_branch_window, 'tp', split_axis=1, concat_axis=0, tiled=...]
    unnamed x45 -> x40, local copies, waits for them, and re-layouts: 5.36 us -> 3.08 us
  transfers between devices with their start and end apart: 5 -> 5, of which waited for: 2 -> 1; matrix products, arithmetic and copies ran while one was open for 18% -> 33% of each run, Pallas kernels for 0% -> 0%
where the time goes in v1:
time: 157 us; the launch traced here: 156 us
  blocking collectives  52.9 us (34%)
  matrix products  35.8 us (23%)
  waiting for transfers between devices  20.1 us (13%)
  starting transfers between devices  13.9 us (9%)
  between operations  13.7 us (9%)
  other arithmetic  12.7 us (8%)
  local copies, waits for them, and re-layouts  6.99 us (4%)
    all_gather x1, blocking collectives, on_device(): lax.all_gather(rope_rows, 'sp', axis=0, tiled=True)  34.6 us
    dot_general x14, matrix products, project(): return jnp.dot(left, right, preferred_element_type=jnp.float32)  27.7 us
    all_to_all x1, waiting for transfers between devices, on_device(): lax.all_to_all(w_branch_latent, 'tp', split_axis=1, concat_axis=0, tiled=...  19.4 us
    all_gather x1, blocking collectives, on_device(): lax.all_gather(window_out, 'tp', axis=1, tiled=True)  9.54 us
    all_gather x1, blocking collectives, on_device(): lax.all_gather(latent_out, 'tp', axis=1, tiled=True)  8.72 us
    ppermute x1, starting transfers between devices, from_behind(): return lax.ppermute(shard, axis, pairs)  5.23 us
    all_to_all x1, starting transfers between devices, on_device(): lax.all_to_all(w_branch_latent, 'tp', split_axis=1, concat_axis=0, tiled=...  4.4 us
    all_to_all x1, starting transfers between devices, on_device(): lax.all_to_all(jnp.stack(jnp.split(w_branch_window, lax.axis_size('tp'),...  4.24 us
  transfers between devices with their start and end apart: 5, of which 1 were waited for; matrix products, arithmetic and copies ran while one was open for 33% of the time, Pallas kernels for 0%

profile of v1, /device:TPU:0, one launch (start us, length us, event | category | flops | bytes accessed | tf_op | source)
XLA Modules:
  0.0 156.2 jit_solution(14720153579535562329)
XLA Ops:
  7.3 2.3 %copy.58 = bf16[256,2048]{0,1:T(8,128)(2,1)} copy(bf16[256,2048]{1,0:T(8,128)(2,1)} %param.37) | data formatting | bytes 2097152 | tf_op args[16]
  9.5 4.4 %all-to-all-start.1 = ((bf16[256,4,512]{0,2,1:T(8,128)(2,1)}), bf16[256,4,512]{0,2,1:T(8,128)(2,1)S(1)}, u32[]{:S(2)}, u32[]{:S(2)}) async-start(bf16[256,4,512]{0,2,1:T(8,128)(2,1)} %bitcast.102), calls=%async_computation.1 | async-start | bytes 2097152 | tf_op jit(solution)/shard_map/all_to_all | solution.py:195
  14.0 1.3 slice_bitcast_fusion.3
  15.3 1.1 pad_maximum_fusion
  16.7 19.4 %all-to-all-done.1 = bf16[256,4,512]{0,2,1:T(8,128)(2,1)S(1)} async-done(((bf16[256,4,512]{0,2,1:T(8,128)(2,1)}), bf16[256,4,512]{0,2,1:T(8,128)(2,1)S(1)}, u32[]{:S(2)}, u32[]{:S(2)}) %all-to-all-start.1) | async-done | bytes 1048608 | tf_op jit(solution)/shard_map/all_to_all | solution.py:195
  36.1 4.2 %all-to-all-start = ((bf16[4,256,512]{2,1,0:T(8,128)(2,1)}), bf16[4,256,512]{2,1,0:T(8,128)(2,1)}, u32[]{:S(2)}, u32[]{:S(2)}) async-start(bf16[4,256,512]{2,1,0:T(8,128)(2,1)} %pad_maximum_fusion), calls=%async_computation | async-start | bytes 2097152 | tf_op jit(solution)/shard_map/all_to_all | solution.py:190
  40.4 1.3 copy.59
  41.7 1.9 %fusion.14 = f32[384]{0:T(512)S(1)} fusion(bf16[384,2048]{1,0:T(8,128)(2,1)} %all-gather.3.cloned.1.call-done), kind=kLoop, calls=%fused_computation.22 | loop fusion | flops 2358912 | bytes 1574400 | tf_op jit(solution)/shard_map/reduce_sum | solution.py:25
  44.1 1.1 multiply_reduce_fusion.1
  46.3 2.0 %convolution_convert_fusion.6 = bf16[384,128]{0,1:T(8,128)(2,1)S(1)} fusion(bf16[384,2048]{1,0:T(8,128)(2,1)} %copy-done.2, bf16[2048,128]{1,0:T(8,128)(2,1)S(1)} %copy-done.10), kind=kOutput, calls=%fused_computation.46 | convolution fusion | flops 201375744 | bytes 2195456 | tf_op jit(solution)/shard_map/dot_general | solution.py:49
  48.4 2.0 %convolution_convert_fusion.5 = bf16[384,128]{0,1:T(8,128)(2,1)S(1)} fusion(bf16[384,2048]{1,0:T(8,128)(2,1)} %copy-done.2, bf16[2048,128]{1,0:T(8,128)(2,1)S(1)} %copy-done.11), kind=kOutput, calls=%fused_computation.45 | convolution fusion | flops 201375744 | bytes 2195456 | tf_op jit(solution)/shard_map/dot_general | solution.py:49
  51.1 5.2 %collective-permute-start = (bf16[128,256]{0,1:T(8,128)(2,1)}, bf16[128,256]{0,1:T(8,128)(2,1)}, u32[]{:S(2)}, u32[]{:S(2)}) collective-permute-start(bf16[128,256]{0,1:T(8,128)(2,1)} %pad_maximum_fusion.5), channel_id=1, source_target_pairs={{0,4},{4,8},{8,12},{12,16},{16,20},{20,24},{24,28},{1,5},{5,9},{9,... | collective-permute-start | bytes 196616 | tf_op jit(solution)/shard_map/ppermute | solution.py:19
  56.9 2.4 %convolution_convert_fusion.3 = bf16[384,256]{1,0:T(8,128)(2,1)S(1)} fusion(bf16[384,2048]{1,0:T(8,128)(2,1)} %copy-done.2, bf16[2048,256]{1,0:T(8,128)(2,1)} %param.23), kind=kOutput, calls=%fused_computation.42 | convolution fusion | flops 402751488 | bytes 2818048 | tf_op jit(solution)/shard_map/dot_general | solution.py:49
  59.6 2.1 %fusion.41 = f32[384,64]{0,1:T(8,128)S(1)} fusion(bf16[384,2048]{1,0:T(8,128)(2,1)} %copy-done.2, bf16[2048,64]{0,1:T(8,128)(2,1)S(1)} %copy-done.16), kind=kOutput, calls=%fused_computation.98 | convolution fusion | flops 100663296 | bytes 1933312 | tf_op jit(solution)/shard_map/dot_general | solution.py:49
  62.0 34.6 %all_gather.18 = bf16[3072,64]{0,1:T(8,128)(2,1)} all-gather(bf16[384,64]{0,1:T(8,128)(2,1)S(1)} %pad_maximum_fusion.6), channel_id=1, replica_groups=mesh['sp'=8,'tp'=4] {'sp'}, dimensions={0}, use_global_device_ids=true | all-gather | bytes 442368 | tf_op jit(solution)/shard_map/all_gather | solution.py:173
  96.7 2.7 %multiply_reduce_fusion = (f32[384]{0:T(512)S(1)}, f32[384,512]{1,0:T(8,128)S(1)}) fusion(bf16[384,2048]{1,0:T(8,128)(2,1)S(1)} %copy-done.3, bf16[2048,512]{1,0:T(8,128)(2,1)} %param.27), kind=kOutput, calls=%fused_computation.49 | convolution fusion | flops 805699200 | bytes 4457984 | tf_op jit(solution)/shard_map/dot_general | solution.py:49
  100.3 1.0 convolution_convert_fusion.2
  101.3 2.0 %fusion.24 = f32[384,512]{1,0:T(8,128)} fusion(bf16[384,2048]{1,0:T(8,128)(2,1)S(1)} %copy-done.3, bf16[2048,512]{1,0:T(8,128)(2,1)S(1)} %copy-done.22), kind=kOutput, calls=%fused_computation.39 | convolution fusion | flops 805896192 | bytes 4456448 | tf_op jit(solution)/shard_map/dot_general | solution.py:49
  103.3 2.0 %fusion.22 = f32[384,512]{1,0:T(8,128)} fusion(bf16[384,2048]{1,0:T(8,128)(2,1)S(1)} %copy-done.3, bf16[2048,512]{1,0:T(8,128)(2,1)S(1)} %copy-done.23), kind=kOutput, calls=%fused_computation.37 | convolution fusion | flops 805896192 | bytes 4456448 | tf_op jit(solution)/shard_map/dot_general | solution.py:49
  108.5 9.5 %all_gather.16 = bf16[384,1024]{0,1:T(8,128)(2,1)} all-gather(bf16[384,256]{0,1:T(8,128)(2,1)S(1)} %bitcast.104), channel_id=1, replica_groups=mesh['sp'=8,'tp'=4] {'tp'}, dimensions={1}, use_global_device_ids=true | all-gather | bytes 983040 | tf_op jit(solution)/shard_map/all_gather | solution.py:185
  118.0 15.7 %conditional.1 = (f32[2,384]{1,0:T(2,128)S(1)}, f32[2,384,128]{1,2,0:T(8,128)}) conditional(s32[]{:T(128)} %convert_element_type.75, () %tuple.13, (s32[]{:T(128)}, s32[384]{0:T(512)S(1)}, bf16[3072,512]{1,0:T(8,128)(2,1)}, bf16[512,256]{1,0:T(8,128)(2,1)S(1)}, bf16[384,256]{1,0:T(8,128)(2,1)}, /*index=5*/bf16[3072,64]{0,1:T(8,128)(2,1)}, ...), branch_computations={%region_5.6_spmd, %region_6.9_spmd} | conditional | flops 3146907136 | bytes 87218872 | solution.py:181
  118.1 0.9 iota_compare_fusion
  119.0 3.4 %convolution_convert_fusion.1 = bf16[3072,256]{0,1:T(8,128)(2,1)S(1)} fusion(bf16[3072,512]{1,0:T(8,128)(2,1)} %get-tuple-element.26, bf16[512,256]{1,0:T(8,128)(2,1)S(1)} %get-tuple-element.38), kind=kOutput, calls=%fused_computation.12 | convolution fusion | flops 806092800 | bytes 4980736 | tf_op jit(solution)/shard_map/cond/branch_1_fun/dot_general | solution.py:49
  122.4 1.6 %fusion.10 = f32[2,3072,384]{2,1,0:T(8,128)S(1)} fusion(bf16[3072,2,128]{0,2,1:T(8,128)(2,1)S(1)} %bitcast.98, bf16[384,256]{1,0:T(8,128)(2,1)S(1)} %copy-done.9), kind=kOutput, calls=%fused_computation.14 | convolution fusion | flops 603979776 | bytes 11206656 | tf_op jit(solution)/shard_map/cond/branch_1_fun/qhd,khd->hqk/dot_general | solution.py:142
  124.0 2.4 %fusion.39 = (f32[2,384]{1,0:T(2,128)S(1)}, f32[2,384,3072]{1,2,0:T(8,128)S(1)}) fusion(bf16[384,2,64]{0,2,1:T(8,128)(2,1)S(1)} %copy-done.12, bf16[3072,64]{0,1:T(8,128)(2,1)S(1)} %copy-done.8, f32[2,3072,384]{2,1,0:T(8,128)S(1)} %fusion.10, pred[384,3072]{0,1:T(8,128)(4,1)S(1)} %iota_compare_fusion), kind=kOutput, calls=%fused_computation.96 | convolution fusion | flops 311426304 | bytes 20548608 | tf_op jit(solution)/shard_map/cond/branch_1_fun/qhr,kr->hqk/dot_general | solution.py:148
  126.4 1.0 convolution_convert_fusion
  127.5 3.1 %fusion.4 = f32[2,384,128]{1,2,0:T(8,128)} fusion(bf16[3072,2,128]{0,2,1:T(8,128)(2,1)S(1)} %bitcast.99, f32[2,384,3072]{1,2,0:T(8,128)S(1)} %get-tuple-element.42, f32[2,384]{1,0:T(2,128)S(1)} %broadcast_maximum_fusion, pred[384,3072]{0,1:T(8,128)(4,1)S(1)} %iota_compare_fusion), kind=kOutput, calls=%fused_computation.6 | convolution fusion | flops 611057664 | bytes 12585984 | tf_op jit(solution)/shard_map/cond | solution.py:181
  130.6 3.2 %fusion.3 = f32[2,384]{1,0:T(2,128)S(1)} fusion(f32[2,384,3072]{1,2,0:T(8,128)S(1)} %get-tuple-element.42, f32[2,384]{1,0:T(2,128)S(1)} %broadcast_maximum_fusion, pred[384,3072]{0,1:T(8,128)(4,1)} %copy-done.4), kind=kLoop, calls=%fused_computation.5 | loop fusion | flops 7077120 | bytes 10622976 | tf_op jit(solution)/shard_map/cond/branch_1_fun/reduce_sum | solution.py:157
  133.8 1.1 divide_convert_fusion.2
  134.9 8.7 %all_gather.19 = bf16[384,1024]{0,1:T(8,128)(2,1)S(1)} all-gather(bf16[384,256]{0,1:T(8,128)(2,1)S(1)} %bitcast.106), channel_id=1, replica_groups=mesh['sp'=8,'tp'=4] {'tp'}, dimensions={1}, use_global_device_ids=true | all-gather | bytes 983040 | tf_op jit(solution)/shard_map/all_gather | solution.py:186
  143.7 2.7 %convolution_multiply_fusion = f32[384,512]{1,0:T(8,128)} fusion(f32[384,512]{1,0:T(8,128)} %fusion.24, bf16[384,1024]{0,1:T(8,128)(2,1)S(1)} %all_gather.19, bf16[1024,512]{1,0:T(8,128)(2,1)S(1)} %bitcast.100), kind=kOutput, calls=%fused_computation.28 | convolution fusion | flops 402849792 | bytes 3407872 | tf_op jit(solution)/shard_map/dot_general | solution.py:49
  146.4 3.0 %fusion.25 = bf16[384,512]{1,0:T(8,128)(2,1)} fusion(f32[384,512]{1,0:T(8,128)} %convolution_multiply_fusion, f32[384,512]{1,0:T(8,128)} %fusion.22, bf16[384,1024]{0,1:T(8,128)(2,1)S(1)} %copy-done.7, bf16[1024,512]{1,0:T(8,128)(2,1)} %bitcast.15), kind=kOutput, calls=%fused_computation.40 | convolution fusion | flops 403243008 | bytes 3801088 | tf_op jit(solution)/shard_map/dot_general | solution.py:49
  (97 shorter events, 8.7 us)
Async XLA Ops:
  6.5 37.6 %copy-start = (bf16[2048,512]{1,0:T(8,128)(2,1)S(1)}, bf16[2048,512]{1,0:T(8,128)(2,1)}, u32[]{:S(2)}) copy-start(bf16[2048,512]{1,0:T(8,128)(2,1)} %param.28) | copy-start | bytes 6291460
  6.5 35.2 %all-gather.3.cloned.1.call-start = ((), (), s32[]{:S(2)}) async-start(), calls=%async_computation.2 | async-start | bytes 1966080 | tf_op jit(solution)/shard_map/all_gather | solution.py:112
  9.5 4.4 %copy-start.24 = (f32[4]{0:T(128)S(1)}, f32[4]{0:T(128)}, u32[]{:S(2)}) copy-start(f32[4]{0:T(128)} %param.26) | copy-start | bytes 52
  9.5 26.6 %all-to-all-start.1 = ((bf16[256,4,512]{0,2,1:T(8,128)(2,1)}), bf16[256,4,512]{0,2,1:T(8,128)(2,1)S(1)}, u32[]{:S(2)}, u32[]{:S(2)}) async-start(bf16[256,4,512]{0,2,1:T(8,128)(2,1)} %bitcast.102), calls=%async_computation.1 | async-start | bytes 2097152 | tf_op jit(solution)/shard_map/all_to_all | solution.py:195
  36.1 110.3 %all-to-all-start = ((bf16[4,256,512]{2,1,0:T(8,128)(2,1)}), bf16[4,256,512]{2,1,0:T(8,128)(2,1)}, u32[]{:S(2)}, u32[]{:S(2)}) async-start(bf16[4,256,512]{2,1,0:T(8,128)(2,1)} %pad_maximum_fusion), calls=%async_computation | async-start | bytes 2097152 | tf_op jit(solution)/shard_map/all_to_all | solution.py:190
  40.3 77.7 %all-gather.5.cloned.1.call-start = ((), (), s32[]{:S(2)}) async-start(), calls=%async_computation.3 | async-start | bytes 3538944 | tf_op jit(solution)/shard_map/all_gather | solution.py:172
  40.4 3.3 %copy-start.19 = (f32[2048]{0:T(1024)S(1)}, f32[2048]{0:T(1024)}, u32[]{:S(2)}) copy-start(f32[2048]{0:T(1024)} %param.22) | copy-start | bytes 24580
  41.7 1.9 %copy-start.5 = (bf16[384,2048]{1,0:T(8,128)(2,1)S(1)}, bf16[384,2048]{1,0:T(8,128)(2,1)}, u32[]{:S(2)}) copy-start(bf16[384,2048]{1,0:T(8,128)(2,1)} %all-gather.3.cloned.1.call-done) | copy-start | bytes 4718596
  44.1 1.2 copy-start.2
  44.1 1.2 copy-start.21
  45.3 1.0 copy-start.10
  46.2 2.2 %copy-start.11 = (bf16[2048,128]{1,0:T(8,128)(2,1)S(1)}, bf16[2048,128]{1,0:T(8,128)(2,1)}, u32[]{:S(2)}) copy-start(bf16[2048,128]{1,0:T(8,128)(2,1)} %param.25) | copy-start | bytes 1572868
  51.1 54.9 %collective-permute-start = (bf16[128,256]{0,1:T(8,128)(2,1)}, bf16[128,256]{0,1:T(8,128)(2,1)}, u32[]{:S(2)}, u32[]{:S(2)}) collective-permute-start(bf16[128,256]{0,1:T(8,128)(2,1)} %pad_maximum_fusion.5), channel_id=1, source_target_pairs={{0,4},{4,8},{8,12},{12,16},{16,20},{20,24},{24,28},{1,5},{5,9},{9,... | collective-permute-start | bytes 196616 | tf_op jit(solution)/shard_map/ppermute | solution.py:19
  56.9 2.7 %copy-start.16 = (bf16[2048,64]{0,1:T(8,128)(2,1)S(1)}, bf16[2048,64]{0,1:T(8,128)(2,1)}, u32[]{:S(2)}) copy-start(bf16[2048,64]{0,1:T(8,128)(2,1)} %param.29) | copy-start | bytes 786436
  59.6 37.1 %copy-start.3 = (bf16[384,2048]{1,0:T(8,128)(2,1)S(1)}, bf16[384,2048]{1,0:T(8,128)(2,1)}, u32[]{:S(2)}) copy-start(bf16[384,2048]{1,0:T(8,128)(2,1)} %copy-done.2) | copy-start | bytes 4718596
  96.7 2.7 %copy-start.17 = (bf16[512,128]{1,0:T(8,128)(2,1)S(1)}, bf16[512,128]{1,0:T(8,128)(2,1)}, u32[]{:S(2)}) copy-start(bf16[512,128]{1,0:T(8,128)(2,1)} %param.33) | copy-start | bytes 393220
  96.7 2.7 %copy-start.20 = (f32[512]{0:T(512)S(1)}, f32[512]{0:T(512)}, u32[]{:S(2)}) copy-start(f32[512]{0:T(512)} %param.30) | copy-start | bytes 6148
  99.4 1.0 copy-start.13
  99.4 1.9 %copy-start.22 = (bf16[2048,512]{1,0:T(8,128)(2,1)S(1)}, bf16[2048,512]{1,0:T(8,128)(2,1)}, u32[]{:S(2)}) copy-start(bf16[2048,512]{1,0:T(8,128)(2,1)} %param.39) | copy-start | bytes 6291460
  101.3 2.0 %copy-start.23 = (bf16[2048,512]{1,0:T(8,128)(2,1)S(1)}, bf16[2048,512]{1,0:T(8,128)(2,1)}, u32[]{:S(2)}) copy-start(bf16[2048,512]{1,0:T(8,128)(2,1)} %param.38) | copy-start | bytes 6291460
  105.3 1.6 %copy-start.18 = (bf16[3,128,2,64]{1,3,2,0:T(8,128)(2,1)S(1)}, bf16[3,128,2,64]{1,3,2,0:T(8,128)(2,1)}, u32[]{:S(2)}) copy-start(bf16[3,128,2,64]{1,3,2,0:T(8,128)(2,1)} %copy.52) | copy-start | bytes 294916
  108.3 9.8 %copy-start.14 = (bf16[512,256]{1,0:T(8,128)(2,1)S(1)}, bf16[512,256]{1,0:T(8,128)(2,1)}, u32[]{:S(2)}) copy-start(bf16[512,256]{1,0:T(8,128)(2,1)} %param.34) | copy-start | bytes 786436
  119.0 8.5 %copy-start.4 = (pred[384,3072]{0,1:T(8,128)(4,1)}, pred[384,3072]{0,1:T(8,128)(4,1)S(1)}, u32[]{:S(2)}) copy-start(pred[384,3072]{0,1:T(8,128)(4,1)S(1)} %iota_compare_fusion) | copy-start | bytes 3538948 | tf_op jit(solution)/shard_map/cond
  119.0 3.4 %copy-start.9 = (bf16[384,256]{1,0:T(8,128)(2,1)S(1)}, bf16[384,256]{1,0:T(8,128)(2,1)}, u32[]{:S(2)}) copy-start(bf16[384,256]{1,0:T(8,128)(2,1)} %get-tuple-element.28) | copy-start | bytes 589828 | tf_op jit(solution)/shard_map/cond
  122.3 1.6 %copy-start.8 = (bf16[3072,64]{0,1:T(8,128)(2,1)S(1)}, bf16[3072,64]{0,1:T(8,128)(2,1)}, u32[]{:S(2)}) copy-start(bf16[3072,64]{0,1:T(8,128)(2,1)} %get-tuple-element.29) | copy-start | bytes 1179652 | tf_op jit(solution)/shard_map/cond
  122.4 1.6 %copy-start.12 = (bf16[384,2,64]{0,2,1:T(8,128)(2,1)S(1)}, bf16[384,2,64]{0,2,1:T(8,128)(2,1)}, u32[]{:S(2)}) copy-start(bf16[384,2,64]{0,2,1:T(8,128)(2,1)} %get-tuple-element.30) | copy-start | bytes 294916 | tf_op jit(solution)/shard_map/cond
  124.0 2.5 %copy-start.1 = (bf16[3072,512]{1,0:T(8,128)(2,1)S(1)}, bf16[3072,512]{1,0:T(8,128)(2,1)}, u32[]{:S(2)}) copy-start(bf16[3072,512]{1,0:T(8,128)(2,1)} %get-tuple-element.26) | copy-start | bytes 9437188 | tf_op jit(solution)/shard_map/cond
  124.0 2.5 %copy-start.15 = (bf16[512,256]{1,0:T(8,128)(2,1)S(1)}, bf16[512,256]{1,0:T(8,128)(2,1)}, u32[]{:S(2)}) copy-start(bf16[512,256]{1,0:T(8,128)(2,1)} %get-tuple-element.39) | copy-start | bytes 786436 | tf_op jit(solution)/shard_map/cond
  133.8 9.9 %copy-start.6 = (bf16[4,256,512]{2,1,0:T(8,128)(2,1)S(1)}, bf16[4,256,512]{2,1,0:T(8,128)(2,1)}, u32[]{:S(2)}) copy-start(bf16[4,256,512]{2,1,0:T(8,128)(2,1)} %copy.59) | copy-start | bytes 3145732
  143.6 2.7 %copy-start.7 = (bf16[384,1024]{0,1:T(8,128)(2,1)S(1)}, bf16[384,1024]{0,1:T(8,128)(2,1)}, u32[]{:S(2)}) copy-start(bf16[384,1024]{0,1:T(8,128)(2,1)} %all_gather.16) | copy-start | bytes 2359300
Sparse Core Ops, SparseCore 0:
  8.9 29.3 all-gather.2
  46.3 66.8 all-gather.4
